TPU v7x, 32 devices: a whole 2x2x4 slice. The times are simulated.
32 devices in a mesh: ep: 16 (over z, x, core), tp: 2 (over y).
Axes of the slice: x: 2, y: 2, z: 4, core: 2. Of those that a mesh axis runs over, the one named last changes fastest.
Arguments:
- tokens: bfloat16 [256, 1024], P('ep'), may hold values from -6 to 6
- state: float32 [256, 16, 64, 64], P('ep', 'tp'), may hold values from -6 to 6
- w_recep: bfloat16 [1024, 1024], P(None, 'tp'), may hold values from -0.1875 to 0.1875
- w_key: bfloat16 [1024, 1024], P(None, 'tp'), may hold values from -0.1875 to 0.1875
- w_value: bfloat16 [1024, 1024], P(None, 'tp'), may hold values from -0.1875 to 0.1875
- w_out: bfloat16 [1024, 1024], P('tp'), may hold values from -0.1875 to 0.1875
- decay_base: float32 [1024], P('tp'), may hold values from -5 to 1
- decay_down: bfloat16 [1024, 64], replicated, may hold values from -0.1875 to 0.1875
- decay_up: bfloat16 [64, 1024], P(None, 'tp'), may hold values from -1 to 1
- rate_base: float32 [1024], P('tp'), may hold values from -4 to 4
- rate_down: bfloat16 [1024, 64], replicated, may hold values from -0.1875 to 0.1875
- rate_up: bfloat16 [64, 1024], P(None, 'tp'), may hold values from -1 to 1
- head_gain: float32 [1024], P('tp'), may hold values from 0.1 to 1.9
- first_gain: float32 [1024], replicated, may hold values from 0.2 to 4.8
- expert_gate: bfloat16 [16, 1024, 1408], P('ep', None, 'tp'), may hold values from -0.1875 to 0.1875
- expert_up: bfloat16 [16, 1024, 1408], P('ep', None, 'tp'), may hold values from -0.1875 to 0.1875
- expert_down: bfloat16 [16, 1408, 1024], P('ep', 'tp'), may hold values from -0.078125 to 0.078125
- dense_gate: bfloat16 [2816, 1024], P('ep'), may hold values from -0.1875 to 0.1875
- dense_up: bfloat16 [2816, 1024], P('ep'), may hold values from -0.1875 to 0.1875
- dense_down: bfloat16 [2816, 1024], P('ep', 'tp'), may hold values from -0.21875 to 0.21875
- branch_gate: bfloat16 [1024], replicated, may hold values from -0.1875 to 0.1875
- second_gain: float32 [1024], P('tp'), may hold values from 0.1 to 1.9
- routes: int32 [256, 2], P('ep'), may hold values from 0 to 3, all different within a row; in each aligned block of 16 rows (0 to 15, 16 to 31, ...) at most 16 rows name the same one
- route_weights: float32 [256, 2], P('ep'), may hold values from 0.2 to 1
Outputs:
- layer_output: bfloat16 [256, 1024], P('ep', 'tp')
Inputs may be any that keep to these rules, and one draw needn't show every extreme that they name: `routes`: each row names 2 different experts. In each aligned block of 16 rows no expert is named by more than 16 rows, a bound that some block reaches.
All inputs are finite; a program needn't handle non-finite values.
Results may differ from a plain program's by a relative error of at most 0.018.
Values may be sent and summed in bfloat16 or wider, within the bound.
A program may use at most 64 MiB of HBM per device.

v0:
```python
import jax
import jax.numpy as jnp
from jax import lax
from jax.sharding import PartitionSpec as P

SPLIT = 4


residual_scale = 1.4142135623730951
norm_epsilon = 1e-05
head_epsilon = 0.00064
key_epsilon = 1e-06


def time_mixer(
    tokens,
    state,
    w_recep,
    w_key,
    w_value,
    w_out,
    decay_base,
    decay_down,
    decay_up,
    rate_base,
    rate_down,
    rate_up,
    head_gain,
):
    row_count = tokens.shape[0]
    head_count = state.shape[1]
    head_size = state.shape[3]
    recep = jnp.dot(tokens, w_recep, preferred_element_type=jnp.float32).reshape(
        row_count, head_count, head_size
    )
    key_vecs = jnp.dot(tokens, w_key, preferred_element_type=jnp.float32).reshape(
        row_count, head_count, head_size
    )
    value_vecs = jnp.dot(tokens, w_value, preferred_element_type=jnp.float32).reshape(
        row_count, head_count, head_size
    )
    decay_low = jnp.tanh(jnp.dot(tokens, decay_down, preferred_element_type=jnp.float32)).astype(
        jnp.bfloat16
    )
    decay_pre = decay_base + jnp.dot(decay_low, decay_up, preferred_element_type=jnp.float32)
    log_rate = -jax.nn.softplus(-decay_pre) - 0.5
    decay = jnp.exp(-jnp.exp(log_rate)).reshape(row_count, head_count, head_size)
    rate_low = jnp.dot(tokens, rate_down, preferred_element_type=jnp.float32).astype(jnp.bfloat16)
    in_rate = jax.nn.sigmoid(
        rate_base + jnp.dot(rate_low, rate_up, preferred_element_type=jnp.float32)
    ).reshape(row_count, head_count, head_size)
    unit_keys = key_vecs * lax.rsqrt(jnp.sum(key_vecs * key_vecs, -1, keepdims=True) + key_epsilon)
    removed = jnp.einsum("bhij,bhj->bhi", state, -unit_keys)
    updated = (
        state * decay[:, :, None, :]
        + removed[..., None] * (unit_keys * in_rate)[:, :, None, :]
        + value_vecs[..., None] * key_vecs[:, :, None, :]
    )
    read_out = jnp.einsum("bhij,bhj->bhi", updated, recep)
    centre = jnp.mean(read_out, -1, keepdims=True)
    spread = jnp.mean(jnp.square(read_out - centre), -1, keepdims=True)
    normed = ((read_out - centre) * lax.rsqrt(spread + head_epsilon)).reshape(
        row_count, head_count * head_size
    ) * head_gain
    return jnp.dot(normed.astype(jnp.bfloat16), w_out, preferred_element_type=jnp.float32)


def first_norm(values, gain):
    centre = jnp.mean(values, -1, keepdims=True)
    spread = jnp.mean(jnp.square(values - centre), -1, keepdims=True)
    return ((values - centre) * lax.rsqrt(spread + norm_epsilon) * gain).astype(jnp.bfloat16)


def route_tables(routes, route_weights, experts, capacity):
    expert_hits = (
        routes[:, :, None] == jnp.arange(experts, dtype=jnp.int32)[None, None, :]
    ).astype(jnp.int32)
    row_hits = jnp.sum(expert_hits, 1, dtype=jnp.int32)
    earlier = jnp.cumsum(row_hits, 0, dtype=jnp.int32) - row_hits
    slot_index = jnp.sum(earlier[:, None, :] * expert_hits, 2, dtype=jnp.int32)
    target = routes * capacity + slot_index
    places = jnp.arange(experts * capacity, dtype=jnp.int32)
    slot_match = target[:, :, None] == places[None, None, :]
    dispatch_tokens = jnp.any(slot_match, 1).astype(jnp.bfloat16)
    combine_experts = jnp.sum(jnp.where(slot_match, route_weights[:, :, None], 0.0), 1)
    return (dispatch_tokens, combine_experts)


def shards(
    tokens,
    state,
    w_recep,
    w_key,
    w_value,
    w_out,
    decay_base,
    decay_down,
    decay_up,
    rate_base,
    rate_down,
    rate_up,
    head_gain,
    first_gain,
    expert_gate,
    expert_up,
    expert_down,
    dense_gate,
    dense_up,
    dense_down,
    branch_gate,
    second_gain,
    routes,
    route_weights,
):
    row_count = tokens.shape[0]
    model_width = tokens.shape[1]
    quarter = w_recep.shape[1]
    tp_index = lax.axis_index("tp")
    partial_mix = time_mixer(
        tokens,
        state,
        w_recep,
        w_key,
        w_value,
        w_out,
        decay_base,
        decay_down,
        decay_up,
        rate_base,
        rate_down,
        rate_up,
        head_gain,
    )
    mixed = lax.psum(partial_mix, "tp")
    x_mid = first_norm(residual_scale * tokens.astype(jnp.float32) + mixed, first_gain)
    own_columns = lax.dynamic_slice_in_dim(x_mid, tp_index * quarter, quarter, 1)
    experts = lax.axis_size("ep") // SPLIT
    capacity = min(row_count, max(2, 2 * row_count * routes.shape[1] // experts))
    dispatch_tokens, combine_experts = route_tables(routes, route_weights, experts, capacity)
    packed_rows = lax.dot_general(
        dispatch_tokens, x_mid, (((0,), (0,)), ((), ())), preferred_element_type=jnp.float32
    ).astype(jnp.bfloat16)
    outgoing = jnp.repeat(packed_rows.reshape(experts, capacity, x_mid.shape[1]), SPLIT, axis=0)
    arrived = lax.all_to_all(outgoing, "ep", split_axis=0, concat_axis=0, tiled=True)
    sources = arrived.shape[0]
    slot_count = arrived.shape[1]
    flat_rows = arrived.reshape(sources * slot_count, model_width)
    gate_pre = jnp.dot(flat_rows, expert_gate[0], preferred_element_type=jnp.float32)
    up_pre = jnp.dot(flat_rows, expert_up[0], preferred_element_type=jnp.float32)
    hidden = (jax.nn.silu(gate_pre) * up_pre).astype(jnp.bfloat16)
    partial_out = jnp.dot(hidden, expert_down[0], preferred_element_type=jnp.float32).reshape(
        sources, slot_count, model_width
    )
    summed = lax.psum_scatter(
        partial_out.astype(jnp.bfloat16), "tp", scatter_dimension=2, tiled=True
    ).astype(jnp.float32)
    returned = lax.all_to_all(
        summed.astype(jnp.bfloat16), "ep", split_axis=0, concat_axis=0, tiled=True
    ).astype(summed.dtype)
    expert_out = jnp.sum(returned.reshape(experts, SPLIT, capacity, quarter), 1).reshape(
        experts * capacity, quarter
    )
    routed_part = jnp.dot(
        combine_experts,
        expert_out,
        precision=lax.Precision.HIGHEST,
        preferred_element_type=jnp.float32,
    )
    branch = jax.nn.sigmoid(jnp.dot(x_mid, branch_gate, preferred_element_type=jnp.float32))
    shard_rows = lax.all_gather(x_mid, "ep", axis=0, tiled=True)
    gate_pre = lax.dot_general(
        shard_rows, dense_gate, (((1,), (1,)), ((), ())), preferred_element_type=jnp.float32
    )
    up_pre = lax.dot_general(
        shard_rows, dense_up, (((1,), (1,)), ((), ())), preferred_element_type=jnp.float32
    )
    dense_hidden = (jax.nn.silu(gate_pre) * up_pre).astype(jnp.bfloat16)
    dense_part = lax.psum_scatter(
        jnp.dot(dense_hidden, dense_down, preferred_element_type=jnp.float32),
        "ep",
        scatter_dimension=0,
        tiled=True,
    )
    second_sum = (
        residual_scale * own_columns.astype(jnp.float32)
        + routed_part
        + branch[:, None] * dense_part
    )
    row_sums, square_sums = lax.psum(
        (jnp.sum(second_sum, 1), jnp.sum(second_sum * second_sum, 1)), "tp"
    )
    average = row_sums / model_width
    spread = square_sums / model_width - average * average
    return (
        (second_sum - average[:, None]) * lax.rsqrt(spread + norm_epsilon)[:, None] * second_gain
    ).astype(jnp.bfloat16)


def solution(mesh):
    return jax.shard_map(
        shards,
        mesh=mesh,
        in_specs=(
            P("ep", None),
            P("ep", "tp", None, None),
            P(None, "tp"),
            P(None, "tp"),
            P(None, "tp"),
            P("tp", None),
            P("tp"),
            P(),
            P(None, "tp"),
            P("tp"),
            P(),
            P(None, "tp"),
            P("tp"),
            P(),
            P("ep", None, "tp"),
            P("ep", None, "tp"),
            P("ep", "tp", None),
            P("ep", None),
            P("ep", None),
            P("ep", "tp"),
            P(),
            P("tp"),
            P("ep", None),
            P("ep", None),
        ),
        out_specs=P("ep", "tp"),
        check_vma=False,
    )
```

profile of v0, /device:TPU:0, one launch (start us, length us, event | category | flops | bytes accessed | tf_op | source)
XLA Modules:
  0.0 162.2 jit_solution(11377209794120408051)
XLA Ops:
  6.5 1.6 fusion.56
  8.3 1.2 fusion.32
  9.6 1.5 fusion.59
  11.2 1.3 fusion.49
  12.6 1.5 fusion.58
  14.2 3.5 %fusion.57 = f32[16,8,1,64]{3,2,1,0:T(1,128)S(1)} fusion(f32[16,8,64,1]{2,3,1,0:T(1,128)S(1)} %bitcast.81, f32[16,8,64,64]{3,2,1,0:T(8,128)} %param.25), kind=kOutput, calls=%fused_computation.85 | convolution fusion | flops 1048576 | bytes 2162688 | tf_op jit(solution)/shard_map/bhij,bhj->bhi/dot_general | solution.py:53
  17.8 2.9 %fusion = f32[16,8,1,64]{3,2,1,0:T(1,128)S(1)} fusion(f32[16,8,64,1]{2,3,1,0:T(1,128)S(1)} %bitcast.83, f32[16,8,64,64]{3,2,1,0:T(8,128)S(1)} %copy-done.1, f32[16,8,64]{2,1,0:T(8,128)S(1)} %reshape.96, f32[16,8,64]{2,1,0:T(8,128)S(1)} %mul.177, f32[16,8,64]{2,1,0:T(8,128)S(1)} %get-tuple-element.10, f32[16,8,64]{2,1,0:T(8,128)S(1)} %bitcast.82, ...), kind=kOutput, calls=%fused_computation | convolution fusion | flops 3670016 | bytes 2326528 | tf_op jit(solution)/shard_map/bhij,bhj->bhi/dot_general | solution.py:59
  21.2 2.1 %fusion.51 = f32[16,1024]{1,0:T(8,128)} fusion(bf16[512,1024]{1,0:T(8,128)(2,1)} %param.29, f32[16,512]{1,0:T(8,128)S(1)} %reshape.99, f32[512]{0:T(512)S(1)} %copy-done.7), kind=kOutput, calls=%fused_computation.66 | convolution fusion | flops 16793600 | bytes 1148928 | tf_op jit(solution)/shard_map/dot_general | solution.py:65
  23.7 23.4 %all-reduce.3.cloned.1.call-done = f32[16,1024]{1,0:T(8,128)} async-done(((f32[16,1024]{1,0:T(8,128)}), f32[16,1024]{1,0:T(8,128)}) %all-reduce.3.cloned.1.call-update) | async-done | bytes 65552 | tf_op jit(solution)/shard_map/psum | solution.py:134
  47.2 1.1 fusion.50
  48.2 1.0 multiply_reduce_fusion
  49.3 0.9 multiply_convert_fusion
  50.5 19.7 %all_to_all.10 = bf16[16,16,1024]{2,1,0:T(8,128)(2,1)S(1)} all-to-all(bf16[16,16,1024]{2,1,0:T(8,128)(2,1)S(1)} %bitcast.72), channel_id=1, replica_groups=mesh['ep'=16,'tp'=2] {'ep'}, dimensions={0} | all-to-all | bytes 1048576 | tf_op jit(solution)/shard_map/all_to_all | solution.py:144
  70.2 0.6 fusion.15
  70.8 0.6 fusion.23
  71.6 1.4 fusion.17
  73.1 21.3 %all_gather.3 = bf16[256,1024]{1,0:T(8,128)(2,1)S(1)} all-gather(bf16[16,1024]{1,0:T(8,128)(2,1)S(1)} %multiply_convert_fusion), channel_id=1, replica_groups=mesh['ep'=16,'tp'=2] {'ep'}, dimensions={0}, use_global_device_ids=true | all-gather | bytes 557056 | tf_op jit(solution)/shard_map/all_gather | solution.py:170
  94.8 1.5 fusion.27
  96.3 3.5 %all-to-all-start.1 = ((bf16[16,16,512]{2,1,0:T(8,128)(2,1)}), bf16[16,16,512]{2,1,0:T(8,128)(2,1)S(1)}, u32[]{:S(2)}, u32[]{:S(2)}) async-start(bf16[16,16,512]{2,1,0:T(8,128)(2,1)} %reduce-scatter.3.cloned.1.call-done), calls=%async_computation.2 | async-start | bytes 524288 | tf_op jit(solution)/shard_map/all_to_all | solution.py:157
  100.1 9.7 %all-to-all-done.1 = bf16[16,16,512]{2,1,0:T(8,128)(2,1)S(1)} async-done(((bf16[16,16,512]{2,1,0:T(8,128)(2,1)}), bf16[16,16,512]{2,1,0:T(8,128)(2,1)S(1)}, u32[]{:S(2)}, u32[]{:S(2)}) %all-to-all-start.1) | async-done | bytes 262176 | tf_op jit(solution)/shard_map/all_to_all | solution.py:157
  109.9 39.1 %reduce-scatter.5.cloned.1.call-done = f32[16,512]{1,0:T(8,128)} async-done(((f32[256,512]{1,0:T(8,128)}), f32[16,512]{1,0:T(8,128)}) %reduce-scatter.5.cloned.1.call-update) | async-done | bytes 32784 | tf_op jit(solution)/shard_map/reduce_scatter | solution.py:178
  148.9 1.1 fusion.55
  150.0 4.9 %all-reduce = (f32[16]{0:T(128)S(1)}, f32[16]{0:T(128)S(1)}) all-reduce(f32[16]{0:T(128)S(1)} %get-tuple-element.6, f32[16]{0:T(128)S(1)} %get-tuple-element.5), channel_id=1, replica_groups=mesh['ep'=16,'tp'=2] {'tp'}, use_global_device_ids=true, to_apply=%region_17.18 | all-reduce | flops 32 | bytes 256 | tf_op jit(solution)/shard_map/psum | solution.py:189
  154.9 0.7 multiply_convert_fusion.1
  (68 shorter events, 2.7 us)
Async XLA Ops:
  6.5 65.1 %copy-start = (bf16[1,704,1024]{2,1,0:T(8,128)(2,1)S(1)}, bf16[1,704,1024]{2,1,0:T(8,128)(2,1)}, u32[]{:S(2)}) copy-start(bf16[1,704,1024]{2,1,0:T(8,128)(2,1)} %param.40) | copy-start | bytes 4325380
  6.5 40.6 %all-reduce.3.cloned.1.call-start = ((), (), s32[]{:S(2)}) async-start(), calls=%async_computation.4 | async-start | bytes 131072 | tf_op jit(solution)/shard_map/psum | solution.py:134
  14.1 3.6 %copy-start.1 = (f32[16,8,64,64]{3,2,1,0:T(8,128)S(1)}, f32[16,8,64,64]{3,2,1,0:T(8,128)}, u32[]{:S(2)}) copy-start(f32[16,8,64,64]{3,2,1,0:T(8,128)} %param.25) | copy-start | bytes 6291460
  17.7 3.5 %copy-start.7 = (f32[512]{0:T(512)S(1)}, f32[512]{0:T(512)}, u32[]{:S(2)}) copy-start(f32[512]{0:T(512)} %param.36) | copy-start | bytes 6148
  17.7 5.6 %copy-start.5 = (s32[16,2]{0,1:T(2,128)S(1)}, s32[16,2]{0,1:T(2,128)}, u32[]{:S(2)}) copy-start(s32[16,2]{0,1:T(2,128)} %param.46) | copy-start | bytes 388
  17.7 29.4 %copy-start.2 = (bf16[16,1024]{1,0:T(8,128)(2,1)S(1)}, bf16[16,1024]{1,0:T(8,128)(2,1)}, u32[]{:S(2)}) copy-start(bf16[16,1024]{1,0:T(8,128)(2,1)} %param.24) | copy-start | bytes 98308
  17.8 31.5 %copy-start.6 = (f32[1024]{0:T(1024)S(1)}, f32[1024]{0:T(1024)}, u32[]{:S(2)}) copy-start(f32[1024]{0:T(1024)} %param.37) | copy-start | bytes 12292
  17.8 52.4 %copy-start.3 = (bf16[1,1024,704]{1,2,0:T(8,128)(2,1)S(1)}, bf16[1,1024,704]{1,2,0:T(8,128)(2,1)}, u32[]{:S(2)}) copy-start(bf16[1,1024,704]{1,2,0:T(8,128)(2,1)} %param.38) | copy-start | bytes 4325380
  23.3 73.0 %reduce-scatter.3.cloned.1.call-start = ((), (), s32[]{:S(2)}) async-start(), calls=%async_computation.5 | async-start | bytes 786432 | tf_op jit(solution)/shard_map/reduce_scatter | solution.py:154
  47.2 23.6 %copy-start.11 = (bf16[1,1024,704]{1,2,0:T(8,128)(2,1)S(1)}, bf16[1,1024,704]{1,2,0:T(8,128)(2,1)}, u32[]{:S(2)}) copy-start(bf16[1,1024,704]{1,2,0:T(8,128)(2,1)} %param.39) | copy-start | bytes 4325380
  70.8 23.6 %copy-start.4 = (bf16[176,1024]{1,0:T(8,128)(2,1)S(1)}, bf16[176,1024]{1,0:T(8,128)(2,1)}, u32[]{:S(2)}) copy-start(bf16[176,1024]{1,0:T(8,128)(2,1)} %param.41) | copy-start | bytes 1081348
  70.8 23.9 %copy-start.12 = (bf16[176,1024]{1,0:T(8,128)(2,1)S(1)}, bf16[176,1024]{1,0:T(8,128)(2,1)}, u32[]{:S(2)}) copy-start(bf16[176,1024]{1,0:T(8,128)(2,1)} %param.42) | copy-start | bytes 1081348
  70.8 23.9 %copy-start.13 = (bf16[176,512]{1,0:T(8,128)(2,1)S(1)}, bf16[176,512]{1,0:T(8,128)(2,1)}, u32[]{:S(2)}) copy-start(bf16[176,512]{1,0:T(8,128)(2,1)} %param.43) | copy-start | bytes 540676
  71.4 28.4 %copy-start.8 = (bf16[1024]{0:T(1024)(128)(2,1)S(1)}, bf16[1024]{0:T(1024)(128)(2,1)}, u32[]{:S(2)}) copy-start(bf16[1024]{0:T(1024)(128)(2,1)} %param.44) | copy-start | bytes 6148
  71.4 28.4 %copy-start.10 = (f32[16,2]{0,1:T(2,128)S(1)}, f32[16,2]{0,1:T(2,128)}, u32[]{:S(2)}) copy-start(f32[16,2]{0,1:T(2,128)} %param.47) | copy-start | bytes 388
  71.6 83.3 %copy-start.9 = (f32[512]{0:T(512)S(1)}, f32[512]{0:T(512)}, u32[]{:S(2)}) copy-start(f32[512]{0:T(512)} %param.45) | copy-start | bytes 6148
  73.1 75.9 %reduce-scatter.5.cloned.1.call-start = ((), (), s32[]{:S(2)}) async-start(), calls=%async_computation.6 | async-start | bytes 557056 | tf_op jit(solution)/shard_map/reduce_scatter | solution.py:178
  96.3 13.5 %all-to-all-start.1 = ((bf16[16,16,512]{2,1,0:T(8,128)(2,1)}), bf16[16,16,512]{2,1,0:T(8,128)(2,1)S(1)}, u32[]{:S(2)}, u32[]{:S(2)}) async-start(bf16[16,16,512]{2,1,0:T(8,128)(2,1)} %reduce-scatter.3.cloned.1.call-done), calls=%async_computation.2 | async-start | bytes 524288 | tf_op jit(solution)/shard_map/all_to_all | solution.py:157
Sparse Core Ops, SparseCore 0:
  23.4 23.6 all-reduce.2
  73.2 13.2 reduce-scatter.2
  96.4 52.5 reduce-scatter.4
where the time goes:
time: 163 us; the launch traced here: 162 us
  waiting for transfers between devices  72.3 us (44%)
  blocking collectives  45.9 us (28%)
  matrix products  21.3 us (13%)
  between operations  13.4 us (8%)
  other arithmetic  4.56 us (3%)
  starting transfers between devices  3.63 us (2%)
    reduce_scatter x1, waiting for transfers between devices, shards(): lax.psum_scatter(jnp.dot(dense_hidden, dense_down, preferred_element_type...  39.1 us
    psum x1, waiting for transfers between devices, shards(): mixed = lax.psum(partial_mix, 'tp')  23.4 us
    all_gather x1, blocking collectives, shards(): shard_rows = lax.all_gather(x_mid, 'ep', axis=0, tiled=True)  21.3 us
    all_to_all x1, blocking collectives, shards(): lax.all_to_all(outgoing, 'ep', split_axis=0, concat_axis=0, tiled=True)  19.7 us
    all_to_all x1, waiting for transfers between devices, shards(): lax.all_to_all(summed.astype(jnp.bfloat16), 'ep', split_axis=0, concat_ax...  9.73 us
    psum x1, blocking collectives, shards(): lax.psum((jnp.sum(second_sum, 1), jnp.sum(second_sum * second_sum, 1)), '...  4.93 us
    all_to_all x1, starting transfers between devices, shards(): lax.all_to_all(summed.astype(jnp.bfloat16), 'ep', split_axis=0, concat_ax...  3.54 us
    dot_general x1, matrix products, time_mixer(): removed = jnp.einsum('bhij,bhj->bhi', state, -unit_keys)  3.51 us
  transfers between devices with their start and end apart: 4, of which 3 were waited for; matrix products, arithmetic and copies ran while one was open for 1% of the time, Pallas kernels for 0%

commit v1 on v0

v1 whole, which is shorter than its diff:
```python
import functools

import jax
import jax.numpy as jnp
from jax import lax
from jax.experimental import pallas as pl
from jax.experimental.pallas import tpu as pltpu
from jax.sharding import PartitionSpec as P

SPLIT = 4
CORES = 2
LANES = 128

residual_scale = 1.4142135623730951
norm_epsilon = 1e-05
head_epsilon = 0.00064
key_epsilon = 1e-06
decay_scale = 0.6065306597126334

F32 = jnp.float32
BF16 = jnp.bfloat16
MESH = pl.DeviceIdType.MESH
NT = (((1,), (1,)), ((), ()))


def dot(a, b):
    return jnp.dot(a, b, preferred_element_type=F32)


def dot_nt(a, b):
    return lax.dot_general(a, b, NT, preferred_element_type=F32)


def layer_kernel(
    ep,
    tp,
    tokens,
    decay_base,
    rate_base,
    head_gain,
    first_gain,
    branch_gate,
    second_gain,
    routes,
    route_weights,
    state_h,
    w_recep_h,
    w_key_h,
    w_value_h,
    w_out_h,
    decay_down_h,
    decay_up_h,
    rate_down_h,
    rate_up_h,
    gate_h,
    up_h,
    down_h,
    dgate_h,
    dup_h,
    ddown_h,
    out,
    state,
    w_recep,
    w_key,
    w_value,
    w_out,
    decay_down,
    decay_up,
    rate_down,
    rate_up,
    gate,
    up,
    down,
    dgate,
    dup,
    ddown,
    mix_send,
    mix_recv,
    xall,
    core_send,
    core_recv,
    plane_send,
    plane_recv,
    line_send,
    line_recv,
    stat_send,
    stat_recv,
    load_sem,
    mix_sems,
    zag_sems,
    xag_sems,
    cag_sems,
    core_sems,
    plane_sems,
    line_sems,
    stat_sems,
):
    rows, width = tokens.shape
    quarter = w_recep.shape[1]
    heads, size = state.shape[1], state.shape[3]
    side = tp
    layers = ep // (side * CORES)
    plane = tp * side
    experts = ep // SPLIT

    me = lax.axis_index("ep")
    mt = lax.axis_index("tp")
    mc = me % CORES
    mx = (me // CORES) % side
    mz = me // (CORES * side)

    def at(z, x, c):
        return (z * side + x) * CORES + c

    pairs = (
        (w_key_h, w_key),
        (decay_down_h, decay_down),
        (rate_down_h, rate_down),
        (decay_up_h, decay_up),
        (rate_up_h, rate_up),
        (w_recep_h, w_recep),
        (w_value_h, w_value),
        (state_h, state),
        (w_out_h, w_out),
        (gate_h, gate),
        (up_h, up),
        (dgate_h, dgate),
        (dup_h, dup),
        (down_h, down),
        (ddown_h, ddown),
    )
    loads = {}
    for n, (src, dst) in enumerate(pairs):
        copy = pltpu.make_async_copy(src, dst, load_sem.at[n])
        copy.start()
        loads[n] = copy

    def peer(e, t):
        return {"ep": e, "tp": t}

    greeted = []
    for d in range(1, layers):
        greeted.append(peer(at((mz + d) % layers, mx, mc), mt))
    for d in range(1, plane):
        m = (mt * side + mx + d) % plane
        greeted.append(peer(at(mz, m % side, mc), m // side))
    greeted.append(peer(at(mz, mx, 1 - mc), mt))
    barrier = pltpu.get_barrier_semaphore()
    for who in greeted:
        pl.semaphore_signal(barrier, inc=1, device_id=who, device_id_type=MESH)

    sent = []

    def send(src, dst, sems, who):
        copy = pltpu.make_async_remote_copy(
            src_ref=src,
            dst_ref=dst,
            send_sem=sems.at[0],
            recv_sem=sems.at[1],
            device_id=who,
            device_id_type=MESH,
        )
        copy.start()
        sent.append(copy)
        return copy

    tok = tokens[...]
    loads[0].wait()
    key_all = dot(tok, w_key[...])
    for n in (1, 2, 3, 4):
        loads[n].wait()
    decay_low = jnp.tanh(dot_nt(tok, decay_down[...])).astype(BF16)
    decay_pre = decay_base[...] + dot(decay_low, decay_up[...])
    decay_all = jnp.exp(-decay_scale * jax.nn.sigmoid(decay_pre))
    rate_low = dot_nt(tok, rate_down[...]).astype(BF16)
    rate_all = jax.nn.sigmoid(rate_base[...] + dot(rate_low, rate_up[...]))
    loads[5].wait()
    recep_all = dot(tok, w_recep[...])
    loads[6].wait()
    value_all = dot(tok, w_value[...])
    loads[7].wait()
    per = LANES // size
    row_id = lax.broadcasted_iota(jnp.int32, (2 * rows, LANES), 0) % rows
    lane_tok = lax.broadcasted_iota(jnp.int32, (2 * rows, LANES), 1) // size
    normed = []
    for h in range(heads):
        cut = slice(h * size, (h + 1) * size)
        k = key_all[:, cut]
        r = recep_all[:, cut]
        v = value_all[:, cut]
        unit = k * lax.rsqrt(jnp.sum(k * k, -1, keepdims=True) + key_epsilon)
        probe = jnp.concatenate([unit, decay_all[:, cut] * r], 0).astype(BF16)
        block = state[:, h].reshape(rows * size, size).astype(BF16)
        cross = dot_nt(probe, block)
        folded = jnp.zeros((2 * rows, LANES), F32)
        for g in range(rows * size // LANES):
            part = cross[:, g * LANES : (g + 1) * LANES]
            folded = folded + jnp.where(row_id == g * per + lane_tok, part, 0.0)
        own = folded[:, :size]
        for g in range(1, per):
            own = own + folded[:, g * size : (g + 1) * size]
        c1 = jnp.sum(unit * rate_all[:, cut] * r, -1, keepdims=True)
        c2 = jnp.sum(k * r, -1, keepdims=True)
        read = own[rows:] - own[:rows] * c1 + v * c2
        read = read - jnp.mean(read, -1, keepdims=True)
        spread = jnp.mean(read * read, -1, keepdims=True)
        normed.append(read * lax.rsqrt(spread + head_epsilon))
    head_out = (jnp.concatenate(normed, 1) * head_gain[...]).astype(BF16)
    loads[8].wait()
    mix_send[...] = dot(head_out, w_out[...]).astype(BF16)

    pl.semaphore_wait(barrier, len(greeted))
    copies = []
    for d in range(1, tp):
        copies.append(
            send(mix_send, mix_recv.at[d - 1], mix_sems.at[d - 1], peer(me, (mt + d) % tp))
        )

    half = LANES // 2
    lane = lax.broadcasted_iota(jnp.int32, (rows, LANES), 1)
    names = routes[...]
    weights = route_weights[...]
    place = lax.broadcasted_iota(jnp.int32, (LANES, rows), 0)
    spots = jnp.zeros((LANES, rows), F32)
    for k in range(names.shape[0]):
        spots = spots + jnp.where(place % half == names[k : k + 1], weights[k : k + 1], 0.0)
    high = spots.astype(BF16).astype(F32)
    spots = jnp.where(place < half, high, spots - high).astype(BF16)
    one = lax.broadcasted_iota(jnp.int32, (rows, rows), 0) == lax.broadcasted_iota(
        jnp.int32, (rows, rows), 1
    )
    extra = dot_nt(jnp.where(one, 1.0, 0.0).astype(BF16), spots)

    total = residual_scale * tok.astype(F32) + mix_send[...].astype(F32)
    for d in range(1, tp):
        copies[d - 1].wait_recv()
        total = total + mix_recv[d - 1].astype(F32)
    total = total - jnp.mean(total, -1, keepdims=True)
    spread = jnp.mean(total * total, -1, keepdims=True)
    x_mid = (total * lax.rsqrt(spread + norm_epsilon) * first_gain[...]).astype(BF16)
    branch = jax.nn.sigmoid(
        jnp.sum(x_mid.astype(F32) * branch_gate[...].astype(F32).reshape(1, width), -1, keepdims=True)
    )
    high = branch.astype(BF16).astype(F32)
    extra = jnp.where(lane == experts, high, extra)
    extra = jnp.where(lane == half + experts, branch - high, extra).astype(BF16)
    xall[me, :, :width] = x_mid
    xall[me, :, width:] = extra

    def gather_wait(kind, d, n):
        sems = {"z": zag_sems, "x": xag_sems, "c": cag_sems}[kind]
        sem = sems.at[d - 1] if kind == "z" else sems.at[d, n]
        pltpu.make_async_remote_copy(
            src_ref=xall.at[me],
            dst_ref=xall.at[me],
            send_sem=sem.at[0],
            recv_sem=sem.at[1],
            device_id=peer(at(mz, mx, 1 - mc), mt),
            device_id_type=MESH,
        ).wait_recv()

    for d in range(1, layers):
        send(
            xall.at[me],
            xall.at[me],
            zag_sems.at[d - 1],
            peer(at((mz + d) % layers, mx, mc), mt),
        )

    def forward_line(d):
        b = at((mz + layers - d) % layers, mx, mc)
        if d:
            gather_wait("z", d, 0)
        for n in range(1, side):
            send(
                xall.at[b],
                xall.at[b],
                xag_sems.at[d, n - 1],
                peer(at(mz, (mx + n) % side, mc), mt),
            )
        send(xall.at[b], xall.at[b], cag_sems.at[d, 0], peer(at(mz, mx, 1 - mc), mt))

    def forward_side(d):
        for n in range(1, side):
            b = at((mz + layers - d) % layers, (mx + side - n) % side, mc)
            gather_wait("x", d, n - 1)
            send(xall.at[b], xall.at[b], cag_sems.at[d, n], peer(at(mz, mx, 1 - mc), mt))

    for d in range(layers):
        forward_line(d)
        if d:
            forward_side(d - 1)
    forward_side(layers - 1)

    count = side * CORES * rows
    expert = me // SPLIT
    lane_c = lax.broadcasted_iota(jnp.int32, (count, LANES), 1) % half

    def compute(d):
        z = (mz + layers - d) % layers
        first = at(z, 0, 0)
        for n in range(side):
            gather_wait("c", d, n)
        if d == 0:
            for n in range(9, 15):
                loads[n].wait()
        blocks = xall[pl.ds(first, side * CORES), :, :]
        flat = blocks.reshape(count, width + LANES)
        x = flat[:, :width]
        tail = flat[:, width:].astype(F32)
        weight = jnp.sum(jnp.where(lane_c == expert, tail, 0.0), -1, keepdims=True)
        branch_c = jnp.sum(jnp.where(lane_c == experts, tail, 0.0), -1, keepdims=True)
        hidden = (jax.nn.silu(dot_nt(x, gate[...])) * dot_nt(x, up[...])).astype(BF16)
        dense = (jax.nn.silu(dot_nt(x, dgate[...])) * dot_nt(x, dup[...])).astype(BF16)
        dense_out = dot(dense, ddown[...]) * branch_c
        for q in range(tp):
            part = dot(hidden, down[:, q * quarter : (q + 1) * quarter]) * weight
            part = part + jnp.where(mt == q, dense_out, 0.0)
            part = part.astype(BF16).reshape(side, CORES, rows, quarter)
            for x_to in range(side):
                for c_to in range(CORES):
                    core_send[d, c_to, q * side + x_to] = part[x_to, c_to]
        return send(
            core_send.at[d, 1 - mc],
            core_recv.at[d],
            core_sems.at[d],
            peer(at(mz, mx, 1 - mc), mt),
        )

    def plane_step(d, copy):
        copy.wait_recv()
        plane_send[d] = (core_send[d, mc].astype(F32) + core_recv[d].astype(F32)).astype(BF16)
        out_copies = []
        for n in range(1, plane):
            m = (mt * side + mx + n) % plane
            out_copies.append(
                send(
                    plane_send.at[d, m],
                    plane_recv.at[d, n - 1],
                    plane_sems.at[d, n - 1],
                    peer(at(mz, m % side, mc), m // side),
                )
            )
        return out_copies

    def line_step(d, in_copies):
        acc = plane_send[d, mt * side + mx].astype(F32)
        for n in range(1, plane):
            in_copies[n - 1].wait_recv()
            acc = acc + plane_recv[d, n - 1].astype(F32)
        if d == 0:
            return acc
        line_send[d - 1] = acc.astype(BF16)
        return send(
            line_send.at[d - 1],
            line_recv.at[d - 1],
            line_sems.at[d - 1],
            peer(at((mz + layers - d) % layers, mx, mc), mt),
        )

    core_out, plane_out, line_out = {}, {}, {}
    for d in range(layers + 2):
        if d < layers:
            core_out[d] = compute(d)
        if 0 <= d - 1 < layers:
            plane_out[d - 1] = plane_step(d - 1, core_out[d - 1])
        if 0 <= d - 2 < layers:
            line_out[d - 2] = line_step(d - 2, plane_out[d - 2])

    columns = pl.ds(pl.multiple_of(mt * quarter, quarter), quarter)
    second = residual_scale * xall[me, :, columns].astype(F32) + line_out[0]
    for d in range(1, layers):
        line_out[d].wait_recv()
        second = second + line_recv[d - 1].astype(F32)

    stat = jnp.where(
        lane == 0,
        jnp.sum(second, -1, keepdims=True),
        jnp.where(lane == 1, jnp.sum(second * second, -1, keepdims=True), 0.0),
    )
    stat_send[...] = stat
    copies = []
    for d in range(1, tp):
        copies.append(
            send(stat_send, stat_recv.at[d - 1], stat_sems.at[d - 1], peer(me, (mt + d) % tp))
        )
    for d in range(1, tp):
        copies[d - 1].wait_recv()
        stat = stat + stat_recv[d - 1]
    average = stat[:, 0:1] / width
    spread = stat[:, 1:2] / width - average * average
    out[...] = (
        (second - average) * lax.rsqrt(spread + norm_epsilon) * second_gain[...]
    ).astype(BF16)
    for copy in sent:
        copy.wait_send()


def shards(
    tokens,
    state,
    w_recep,
    w_key,
    w_value,
    w_out,
    decay_base,
    decay_down,
    decay_up,
    rate_base,
    rate_down,
    rate_up,
    head_gain,
    first_gain,
    expert_gate,
    expert_up,
    expert_down,
    dense_gate,
    dense_up,
    dense_down,
    branch_gate,
    second_gain,
    routes,
    route_weights,
):
    ep, tp = lax.axis_size("ep"), lax.axis_size("tp")
    rows, width = tokens.shape
    quarter = w_recep.shape[1]
    side = tp
    layers = ep // (side * CORES)
    plane = tp * side
    large = (
        state,
        w_recep,
        w_key,
        w_value,
        w_out,
        decay_down.T,
        decay_up,
        rate_down.T,
        rate_up,
        expert_gate[0].T,
        expert_up[0].T,
        expert_down[0],
        dense_gate,
        dense_up,
        dense_down,
    )
    small = (
        tokens,
        decay_base[None],
        rate_base[None],
        head_gain[None],
        first_gain[None],
        branch_gate,
        second_gain[None],
        routes.T,
        route_weights.T,
    )
    dma = pltpu.SemaphoreType.DMA
    return pl.pallas_call(
        functools.partial(layer_kernel, ep, tp),
        out_shape=jax.ShapeDtypeStruct((rows, quarter), BF16),
        in_specs=[pl.BlockSpec(memory_space=pltpu.VMEM)] * len(small)
        + [pl.BlockSpec(memory_space=pl.ANY)] * len(large),
        out_specs=pl.BlockSpec(memory_space=pltpu.VMEM),
        scratch_shapes=[pltpu.VMEM(a.shape, a.dtype) for a in large]
        + [
            pltpu.VMEM((rows, width), BF16),
            pltpu.VMEM((tp - 1, rows, width), BF16),
            pltpu.VMEM((ep, rows, width + LANES), BF16),
            pltpu.VMEM((layers, CORES, plane, rows, quarter), BF16),
            pltpu.VMEM((layers, plane, rows, quarter), BF16),
            pltpu.VMEM((layers, plane, rows, quarter), BF16),
            pltpu.VMEM((layers, plane - 1, rows, quarter), BF16),
            pltpu.VMEM((layers - 1, rows, quarter), BF16),
            pltpu.VMEM((layers - 1, rows, quarter), BF16),
            pltpu.VMEM((rows, LANES), F32),
            pltpu.VMEM((tp - 1, rows, LANES), F32),
            dma((len(large),)),
            dma((tp - 1, 2)),
            dma((layers - 1, 2)),
            dma((layers, side - 1, 2)),
            dma((layers, side, 2)),
            dma((layers, 2)),
            dma((layers, plane - 1, 2)),
            dma((layers - 1, 2)),
            dma((tp - 1, 2)),
        ],
        compiler_params=pltpu.CompilerParams(collective_id=0, has_side_effects=True),
    )(*small, *large)


def solution(mesh):
    return jax.shard_map(
        shards,
        mesh=mesh,
        in_specs=(
            P("ep", None),
            P("ep", "tp", None, None),
            P(None, "tp"),
            P(None, "tp"),
            P(None, "tp"),
            P("tp", None),
            P("tp"),
            P(),
            P(None, "tp"),
            P("tp"),
            P(),
            P(None, "tp"),
            P("tp"),
            P(),
            P("ep", None, "tp"),
            P("ep", None, "tp"),
            P("ep", "tp", None),
            P("ep", None),
            P("ep", None),
            P("ep", "tp"),
            P(),
            P("tp"),
            P("ep", None),
            P("ep", None),
        ),
        out_specs=P("ep", "tp"),
        check_vma=False,
    )
```

time: 163 us -> 42.6 us (0.26)
  waiting for transfers between devices: 72.3 us -> 0 us
  blocking collectives: 45.9 us -> 0 us
  Pallas kernels: 0 us -> 41 us
  matrix products: 21.3 us -> 0 us
  between operations: 13.4 us -> 0.01 us
  other arithmetic: 4.56 us -> 0 us
  starting transfers between devices: 3.63 us -> 0 us
    pallas_call x0 -> x1, Pallas kernels: none -> 41 us  [shards(): pl.pallas_call(functools.partial(layer_kernel, ep, tp), out_shape=jax.Sha...]
    reduce_scatter x2 -> x0, waiting for transfers between devices: 39.1 us -> none  [the longest x1 39.1 us: shards(): lax.psum_scatter(jnp.dot(dense_hidden, dense_down, preferred_element_type...]
    psum x1 -> x0, waiting for transfers between devices: 23.4 us -> none  [shards(): mixed = lax.psum(partial_mix, 'tp')]
    dot_general x16 -> x0, matrix products: 21.3 us -> none  [the longest x1 3.51 us: time_mixer(): removed = jnp.einsum('bhij,bhj->bhi', state, -unit_keys)]
    all_gather x1 -> x0, blocking collectives: 21.3 us -> none  [shards(): shard_rows = lax.all_gather(x_mid, 'ep', axis=0, tiled=True)]
    all_to_all x1 -> x0, blocking collectives: 19.7 us -> none  [shards(): lax.all_to_all(outgoing, 'ep', split_axis=0, concat_axis=0, tiled=True)]
    all_to_all x1 -> x0, waiting for transfers between devices: 9.73 us -> none  [shards(): lax.all_to_all(summed.astype(jnp.bfloat16), 'ep', split_axis=0, concat_ax...]
    psum x1 -> x0, blocking collectives: 4.93 us -> none  [shards(): lax.psum((jnp.sum(second_sum, 1), jnp.sum(second_sum * second_sum, 1)), '...]
  transfers between devices with their start and end apart: 4 -> 0, of which waited for: 3 -> 0; matrix products, arithmetic and copies ran while one was open for 1% -> 0% of each run, Pallas kernels for 0% -> 0%
where the time goes in v1:
time: 42.6 us; the launch traced here: 42.4 us
  Pallas kernels  41 us (96%)
  local copies, waits for them, and re-layouts  1.32 us (3%)
    pallas_call x1, Pallas kernels, shards(): pl.pallas_call(functools.partial(layer_kernel, ep, tp), out_shape=jax.Sha...  41 us
    unnamed x1, local copies, waits for them, and re-layouts  1.32 us

profile of v1, /device:TPU:0, one launch (start us, length us, event | category | flops | bytes accessed | tf_op | source)
XLA Modules:
  0.0 42.4 jit_solution(6265573362430753045)
XLA Ops:
  0.0 41.0 %shard_map.226 = bf16[16,512]{1,0:T(8,128)(2,1)} custom-call(bf16[16,1024]{1,0:T(8,128)(2,1)} %tokens.1, f32[1,512]{1,0:T(1,128)} %bitcast.22, f32[1,512]{1,0:T(1,128)} %bitcast.23, f32[1,512]{1,0:T(1,128)} %bitcast.24, f32[1,1024]{1,0:T(1,128)} %bitcast.21, bf16[1024]{0:T(1024)(128)(2,1)} %branch_gate.1, f32[1,512]{1,0:T(1,128)} %bitcast.25, ...), custom_call_target="tpu_custom_call" | custom-call | tf_op jit(solution)/shard_map/pallas_call | solution.py:460
  41.1 1.3 %copy.26 = bf16[16,512]{1,0:T(8,128)(2,1)} copy(bf16[16,512]{1,0:T(8,128)(2,1)} %shard_map.226) | data formatting | bytes 32768

commit v2 on v1

--- a/solution.py
+++ b/solution.py
@@ -286,12 +286,6 @@
             gather_wait("x", d, n - 1)
             send(xall.at[b], xall.at[b], cag_sems.at[d, n], peer(at(mz, mx, 1 - mc), mt))
 
-    for d in range(layers):
-        forward_line(d)
-        if d:
-            forward_side(d - 1)
-    forward_side(layers - 1)
-
     count = side * CORES * rows
     expert = me // SPLIT
     lane_c = lax.broadcasted_iota(jnp.int32, (count, LANES), 1) % half
@@ -359,13 +353,17 @@
         )
 
     core_out, plane_out, line_out = {}, {}, {}
-    for d in range(layers + 2):
+    for d in range(layers + 4):
         if d < layers:
-            core_out[d] = compute(d)
+            forward_line(d)
         if 0 <= d - 1 < layers:
-            plane_out[d - 1] = plane_step(d - 1, core_out[d - 1])
+            forward_side(d - 1)
         if 0 <= d - 2 < layers:
-            line_out[d - 2] = line_step(d - 2, plane_out[d - 2])
+            core_out[d - 2] = compute(d - 2)
+        if 0 <= d - 3 < layers:
+            plane_out[d - 3] = plane_step(d - 3, core_out[d - 3])
+        if 0 <= d - 4 < layers:
+            line_out[d - 4] = line_step(d - 4, plane_out[d - 4])
 
     columns = pl.ds(pl.multiple_of(mt * quarter, quarter), quarter)
     second = residual_scale * xall[me, :, columns].astype(F32) + line_out[0]

time: 42.6 us -> 40.3 us (0.946)
  Pallas kernels: 41 us -> 38.7 us
    pallas_call x1, Pallas kernels: 41 us -> 38.7 us  [shards(): pl.pallas_call(functools.partial(layer_kernel, ep, tp), out_shape=jax.Sha...]
where the time goes in v2:
time: 40.3 us; the launch traced here: 40 us
  Pallas kernels  38.7 us (96%)
  local copies, waits for them, and re-layouts  1.32 us (3%)
    pallas_call x1, Pallas kernels, shards(): pl.pallas_call(functools.partial(layer_kernel, ep, tp), out_shape=jax.Sha...  38.7 us
    unnamed x1, local copies, waits for them, and re-layouts  1.32 us

profile of v2, /device:TPU:0, one launch (start us, length us, event | category | flops | bytes accessed | tf_op | source)
XLA Modules:
  0.0 40.0 jit_solution(10741566814044725638)
XLA Ops:
  0.0 38.7 %shard_map.226 = bf16[16,512]{1,0:T(8,128)(2,1)} custom-call(bf16[16,1024]{1,0:T(8,128)(2,1)} %tokens.1, f32[1,512]{1,0:T(1,128)} %bitcast.22, f32[1,512]{1,0:T(1,128)} %bitcast.23, f32[1,512]{1,0:T(1,128)} %bitcast.24, f32[1,1024]{1,0:T(1,128)} %bitcast.21, bf16[1024]{0:T(1024)(128)(2,1)} %branch_gate.1, f32[1,512]{1,0:T(1,128)} %bitcast.25, ...), custom_call_target="tpu_custom_call" | custom-call | tf_op jit(solution)/shard_map/pallas_call | solution.py:458
  38.7 1.3 %copy.26 = bf16[16,512]{1,0:T(8,128)(2,1)} copy(bf16[16,512]{1,0:T(8,128)(2,1)} %shard_map.226) | data formatting | bytes 32768
